TPU v7x, 512 devices: a whole 4x4x16 slice. The times are simulated.
512 devices in a mesh: sp: 32 (over z, core), tp: 16 (over y, x).
Axes of the slice: x: 4, y: 4, z: 16, core: 2. Of those that a mesh axis runs over, the one named last changes fastest.
Arguments:
- query_a: bfloat16 [6144, 2048], P('sp', 'tp'), may hold values from -6 to 6
- key_a: bfloat16 [6144, 2048], P('sp', 'tp'), may hold values from -6 to 6
- value_a: bfloat16 [6144, 2048], P('sp', 'tp'), may hold values from -6 to 6
- query_b: bfloat16 [6144, 2048], P('sp', 'tp'), may hold values from -6 to 6
- key_b: bfloat16 [6144, 2048], P('sp', 'tp'), may hold values from -6 to 6
- value_b: bfloat16 [6144, 2048], P('sp', 'tp'), may hold values from -6 to 6
- stop_a: float32 [6144, 32], P('sp', 'tp'), may hold values from -14 to -1
- stop_b: float32 [6144, 16], P('sp', 'tp'), may hold values from -14 to -1
- out_a: bfloat16 [2048, 2048], P('tp'), may hold values from -4 to 4
- out_b: bfloat16 [2048, 2048], P('tp'), may hold values from -4 to 4
- resid: bfloat16 [6144, 2048], P('sp', 'tp'), may hold values from -20 to 20
- mix_gain: float32 [2048], P('tp'), may hold values from 0.1 to 1.9
- ffn_gain: float32 [2048], P('tp'), may hold values from 0.1 to 1.9
- routes: int32 [6144, 2], P('sp'), may hold values from 0 to 127, all different within a row; in each aligned block of 192 rows (0 to 191, 192 to 383, ...) at most 5 rows name the same one
- gates: float32 [6144, 2], P('sp'), may hold values from 0.25 to 1.5
- exp_gate: bfloat16 [128, 2048, 512], P('sp', 'tp'), may hold values from -0.125 to 0.125
- exp_up: bfloat16 [128, 2048, 512], P('sp', 'tp'), may hold values from -0.125 to 0.125
- exp_down: bfloat16 [128, 512, 2048], P('sp', None, 'tp'), may hold values from -0.25 to 0.25
- sh_gate: bfloat16 [2048, 512], P('tp'), may hold values from -0.125 to 0.125
- sh_up: bfloat16 [2048, 512], P('tp'), may hold values from -0.125 to 0.125
- sh_down: bfloat16 [512, 2048], P(None, 'tp'), may hold values from -4 to 4
Outputs:
- result: bfloat16 [6144, 2048], P('sp', 'tp')
Inputs may be any that keep to these rules, and one draw needn't show every extreme that they name: `routes`: each row names 2 different experts. Within the rows of one index of sp (aligned blocks of 192 rows) no expert is named by more than 5 rows, a bound that some block reaches.
All inputs are finite; a program needn't handle non-finite values.
Results may differ from a plain program's by a relative error of at most 0.02.
Values may be sent and summed in bfloat16 or wider, within the bound.
A program may use at most 64 MiB of HBM per device.

v0:
```python
import jax
import jax.numpy as jnp
from jax import lax
from jax.sharding import Mesh
from jax.sharding import PartitionSpec as P

D = 2048
TP = ("tp_0", "tp_1")
epsilon = 1e-06


def cut_along(x, dim, size):
    before, after = (x.shape[:dim], x.shape[dim + 1 :])
    return jnp.moveaxis(x.reshape(*before, size, -1, *after), dim, 0)


def sum_at_owner(x, axis, dim):
    tiles = cut_along(x, dim, lax.axis_size(axis))
    arrived = lax.all_to_all(tiles, axis, split_axis=0, concat_axis=0, tiled=True)
    return arrived.astype(jnp.float32).sum(axis=0)


def by_axis(x, axes):
    for axis in axes:
        x = lax.psum(x, axis)
    return x


def suffix_sums(failing):
    width = failing.shape[-1]
    pieces = width // width
    shaped = failing.reshape(failing.shape[:-1] + (pieces, width))
    places = jnp.arange(width)
    upper = (places[:, None] > places[None, :]).astype(jnp.float32)
    inner = jnp.matmul(shaped, upper)
    return inner.reshape(failing.shape)


def stick_block(state, queries, keyset, causal):
    outputs, carried = state
    new_out = []
    new_carry = []
    for group in range(2):
        query, stop, scale = queries[group]
        keys = keyset[2 * group]
        values = keyset[2 * group + 1]
        scores = jnp.einsum("qhd,khd->hqk", query, keys, preferred_element_type=jnp.float32)
        scores = scores * scale + jnp.transpose(stop)[:, :, None]
        failing = jax.nn.log_sigmoid(-scores)
        if causal is not None:
            failing = jnp.where(causal, failing, 0.0)
        after = suffix_sums(failing) + carried[group][:, :, None]
        weight = jnp.exp(jax.nn.log_sigmoid(scores) + after)
        if causal is not None:
            weight = jnp.where(causal, weight, 0.0)
        added = jnp.einsum(
            "hqk,khe->qhe", weight.astype(jnp.bfloat16), values, preferred_element_type=jnp.float32
        )
        new_out.append(outputs[group] + added)
        new_carry.append(carried[group] + jnp.sum(failing, axis=-1))
    return (tuple(new_out), tuple(new_carry))


def empty_state(count, heads_a, size_a, heads_b, size_b):
    return (
        (
            jnp.zeros((count, heads_a, size_a), jnp.float32),
            jnp.zeros((count, heads_b, size_b), jnp.float32),
        ),
        (jnp.zeros((heads_a, count), jnp.float32), jnp.zeros((heads_b, count), jnp.float32)),
    )


def joined_rows(state, width_a, width_b):
    count = state[0][0].shape[0]
    return jnp.concatenate(
        [
            state[0][0].astype(jnp.bfloat16).reshape(count, width_a),
            state[0][1].astype(jnp.bfloat16).reshape(count, width_b),
        ],
        axis=1,
    )


def shards(
    query_a,
    key_a,
    value_a,
    query_b,
    key_b,
    value_b,
    stop_a,
    stop_b,
    out_a,
    out_b,
    resid,
    mix_gain,
    ffn_gain,
    routes,
    gates,
    exp_gate,
    exp_up,
    exp_down,
    sh_gate,
    sh_up,
    sh_down,
):
    rows = query_a.shape[0]
    heads_a = stop_a.shape[1]
    heads_b = stop_b.shape[1]
    width_a = query_a.shape[1]
    width_b = query_b.shape[1]
    size_a = width_a // heads_a
    size_b = width_b // heads_b

    def unpack(joined):
        count = joined.shape[0]
        return (
            joined[:, :width_a].reshape(count, heads_a, size_a),
            joined[:, width_a : 2 * width_a].reshape(count, heads_a, size_a),
            joined[:, 2 * width_a : 2 * width_a + width_b].reshape(count, heads_b, size_b),
            joined[:, 2 * width_a + width_b :].reshape(count, heads_b, size_b),
        )

    joined_local = jnp.concatenate([key_a, value_a, key_b, value_b], axis=1)
    places = jnp.arange(rows)
    position = lax.axis_index("sp")
    n_sp = lax.axis_size("sp")
    count = query_a.shape[0]
    queries = (
        (query_a.reshape(count, heads_a, size_a), stop_a, size_a ** (-0.5)),
        (query_b.reshape(count, heads_b, size_b), stop_b, size_b ** (-0.5)),
    )
    causal = (places[None, :] < places[:, None])[None]
    state = stick_block(
        empty_state(rows, heads_a, size_a, heads_b, size_b), queries, unpack(joined_local), causal
    )
    gathered = lax.all_gather(joined_local, "sp", axis=0, tiled=True)

    def turn(step, inner_state):
        start = jnp.maximum(position - step, 0) * rows
        piece = lax.dynamic_slice_in_dim(gathered, start, rows, 0)
        return lax.cond(
            position >= step,
            lambda inputs: stick_block(inputs, queries, unpack(piece), None),
            lambda inputs: inputs,
            inner_state,
        )

    state = lax.fori_loop(1, n_sp, turn, state)
    attended = joined_rows(state, width_a, width_b)
    attended_a = attended[:, :width_a]
    attended_b = attended[:, width_a:]
    partial_value = jnp.dot(attended_a, out_a, preferred_element_type=jnp.float32)
    partial_value = partial_value + jnp.dot(attended_b, out_b, preferred_element_type=jnp.float32)
    mixed = sum_at_owner(partial_value.astype(jnp.bfloat16), TP, 1)
    mix_total = by_axis(jnp.sum(mixed * mixed, axis=1), TP)
    branch = mixed * lax.rsqrt(mix_total / D + epsilon)[:, None] * mix_gain[None, :]
    stream = lax.optimization_barrier((resid.astype(jnp.float32) + branch).astype(jnp.bfloat16))
    stream_f = stream.astype(jnp.float32)
    ffn_total = by_axis(jnp.sum(stream_f * stream_f, axis=1), TP)
    normed = (stream_f * lax.rsqrt(ffn_total / D + epsilon)[:, None] * ffn_gain[None, :]).astype(
        jnp.bfloat16
    )
    shared_gate, shared_up = (
        lax.psum(
            jnp.dot(normed, sh_gate, preferred_element_type=jnp.float32).astype(jnp.bfloat16), TP
        ).astype(jnp.float32),
        lax.psum(
            jnp.dot(normed, sh_up, preferred_element_type=jnp.float32).astype(jnp.bfloat16), TP
        ).astype(jnp.float32),
    )
    shared_hidden = (jax.nn.silu(shared_gate) * shared_up).astype(jnp.bfloat16)
    shared_out = jnp.dot(shared_hidden, sh_down, preferred_element_type=jnp.float32)
    local_experts = exp_gate.shape[0]
    experts = local_experts * n_sp
    top_count = routes.shape[1]
    capacity = max(1, (3 * rows * top_count + 2 * experts - 1) // (2 * experts))
    flat_routes = routes.reshape(-1)
    onehot = (flat_routes[:, None] == jnp.arange(experts, dtype=jnp.int32)[None, :]).astype(
        jnp.int32
    )
    earlier = jnp.cumsum(onehot, axis=0) - onehot
    slot = flat_routes * capacity + jnp.sum(earlier * onehot, axis=1)
    chooser = (slot[:, None] == jnp.arange(experts * capacity, dtype=jnp.int32)[None, :]).astype(
        jnp.bfloat16
    )
    chooser = jnp.sum(chooser.reshape(rows, top_count, experts * capacity), axis=1)
    outgoing = jnp.einsum("rs,rc->sc", chooser, normed, preferred_element_type=jnp.float32).astype(
        jnp.bfloat16
    )
    outgoing = outgoing.reshape(n_sp, local_experts, capacity, normed.shape[1])
    arrived = lax.all_to_all(outgoing, "sp", split_axis=0, concat_axis=0, tiled=True)
    gate_part = jnp.einsum("segd,edf->segf", arrived, exp_gate, preferred_element_type=jnp.float32)
    up_part = jnp.einsum("segd,edf->segf", arrived, exp_up, preferred_element_type=jnp.float32)
    gate_pre = lax.psum(gate_part.astype(jnp.bfloat16), TP).astype(jnp.float32)
    up_pre = lax.psum(up_part.astype(jnp.bfloat16), TP).astype(jnp.float32)
    hidden = (jax.nn.silu(gate_pre) * up_pre).astype(jnp.bfloat16)
    produced = jnp.einsum("segf,efd->segd", hidden, exp_down, preferred_element_type=jnp.float32)
    returned = lax.all_to_all(
        produced.astype(jnp.bfloat16), "sp", split_axis=0, concat_axis=0, tiled=True
    )
    flat_back = returned.reshape(experts * capacity, returned.shape[3])
    picked = jnp.take(flat_back, slot, axis=0).reshape(rows, top_count, returned.shape[3])
    routed = jnp.sum(gates[:, :, None] * picked.astype(jnp.float32), axis=1)
    moe = routed + shared_out
    result = stream_f + moe
    return result.astype(jnp.bfloat16)


def solution(mesh):
    finer = Mesh(mesh.devices.reshape(mesh.shape["sp"], 4, 4), ("sp", "tp_0", "tp_1"))
    in_specs = (
        P("sp", TP),
        P("sp", TP),
        P("sp", TP),
        P("sp", TP),
        P("sp", TP),
        P("sp", TP),
        P("sp", TP),
        P("sp", TP),
        P(TP, None),
        P(TP, None),
        P("sp", TP),
        P(TP),
        P(TP),
        P("sp", None),
        P("sp", None),
        P("sp", TP, None),
        P("sp", TP, None),
        P("sp", None, TP),
        P(TP, None),
        P(TP, None),
        P(None, TP),
    )
    out_specs = P("sp", TP)
    return jax.shard_map(
        shards, mesh=finer, in_specs=in_specs, out_specs=out_specs, check_vma=False
    )
```

profile of v0, /device:TPU:1, one launch (start us, length us, event | category | flops | bytes accessed | tf_op | source)
XLA Modules:
  0.0 487.4 jit_solution(6028487693172046048)
XLA Ops:
  6.5 1.6 pad_maximum_fusion
  12.0 1.1 fusion.127
  15.3 76.1 %all-gather.2.cloned.1.call-done = bf16[6144,512]{1,0:T(8,128)(2,1)} async-done(((bf16[192,512]{1,0:T(8,128)(2,1)}), bf16[6144,512]{1,0:T(8,128)(2,1)}) %all-gather.2.cloned.1.call-update) | async-done | bytes 6291472 | tf_op jit(solution)/shard_map/all_gather | solution.py:138
  91.4 8.7 %copy.134 = bf16[6144,512]{0,1:T(8,128)(2,1)} copy(bf16[6144,512]{1,0:T(8,128)(2,1)} %all-gather.2.cloned.1.call-done) | data formatting | bytes 12582912 | tf_op jit(solution)/shard_map/while | solution.py:150
  100.1 6.4 %while.19 = (s32[]{:T(128)}, f32[192,2,64]{0,2,1:T(8,128)S(1)}, f32[192,1,128]{2,0,1:T(8,128)S(1)}, f32[2,192]{1,0:T(2,128)S(1)}, f32[1,192]{1,0:T(1,128)S(1)}, ...) while((s32[]{:T(128)}, f32[192,2,64]{0,2,1:T(8,128)S(1)}, ...), condition=%wide.region_7.8_spmd, body=%wide.region_2.7_spmd.sunk | while | flops 83325512 | bytes 2064037 | solution.py:150
  100.1 5.1 %conditional.2 = ((f32[192,2,64]{0,2,1:T(8,128)S(1)}, f32[192,1,128]{2,0,1:T(8,128)S(1)}, f32[2,192]{1,0:T(2,128)S(1)}, f32[1,192]{1,0:T(1,128)S(1)})) conditional(s32[]{:T(128)} %convert_element_type.258, (f32[192,2,64]{0,2,1:T(8,128)S(1)}, f32[192,1,128]{2,0,1:T(8,128)S(1)}, f32[2,192]{1,0:T(2,128)S(1)}, f32[1,192]{1,0:T(1,128)S(1)}) %tuple.58, ...), branch_computations={%region_3.3_spmd, %region_4.6_spmd} | conditional | flops 83325512 | bytes 2063786 | solution.py:143
  102.4 1.3 fusion.43
  103.7 1.5 fusion.13
  109.0 6.7 %all-to-all-start = ((bf16[16,192,128]{2,1,0:T(8,128)(2,1)}), bf16[16,192,128]{2,1,0:T(8,128)(2,1)S(1)}, u32[]{:S(2)}, u32[]{:S(2)}) async-start(bf16[16,192,128]{2,1,0:T(8,128)(2,1)} %bitcast.107), calls=%async_computation | async-start | bytes 1572864 | tf_op jit(solution)/shard_map/all_to_all | solution.py:19
  116.6 9.7 %all-to-all-done = bf16[16,192,128]{2,1,0:T(8,128)(2,1)S(1)} async-done(((bf16[16,192,128]{2,1,0:T(8,128)(2,1)}), bf16[16,192,128]{2,1,0:T(8,128)(2,1)S(1)}, u32[]{:S(2)}, u32[]{:S(2)}) %all-to-all-start) | async-done | bytes 786464 | tf_op jit(solution)/shard_map/all_to_all | solution.py:19
  126.6 6.5 %psum.56 = f32[192]{0:T(256)S(1)} all-reduce(f32[192]{0:T(256)S(1)} %multiply_reduce_fusion.1), channel_id=1, replica_groups=mesh['sp'=32,'tp_0'=4,'tp_1'=4] {'tp_0'}, use_global_device_ids=true, to_apply=%region_10.11 | all-reduce | flops 192 | bytes 1536 | tf_op jit(solution)/shard_map/psum | solution.py:25
  133.1 6.8 %psum.57 = f32[192]{0:T(256)S(1)} all-reduce(f32[192]{0:T(256)S(1)} %psum.56), channel_id=1, replica_groups=mesh['sp'=32,'tp_0'=4,'tp_1'=4] {'tp_1'}, use_global_device_ids=true, to_apply=%region_11.12 | all-reduce | flops 192 | bytes 1536 | tf_op jit(solution)/shard_map/psum | solution.py:25
  140.1 6.5 %psum.58 = f32[192]{0:T(256)S(1)} all-reduce(f32[192]{0:T(256)S(1)} %fusion.130), channel_id=1, replica_groups=mesh['sp'=32,'tp_0'=4,'tp_1'=4] {'tp_0'}, use_global_device_ids=true, to_apply=%region_17.18 | all-reduce | flops 192 | bytes 1536 | tf_op jit(solution)/shard_map/psum | solution.py:25
  146.6 7.1 %psum.59 = f32[192]{0:T(256)S(1)} all-reduce(f32[192]{0:T(256)S(1)} %psum.58), channel_id=1, replica_groups=mesh['sp'=32,'tp_0'=4,'tp_1'=4] {'tp_1'}, use_global_device_ids=true, to_apply=%region_18.19 | all-reduce | flops 192 | bytes 1536 | tf_op jit(solution)/shard_map/psum | solution.py:25
  154.9 161.9 %all-to-all-start.1 = ((bf16[32,4,5,128]{3,1,2,0:T(4,128)(2,1)}), bf16[32,4,5,128]{3,1,2,0:T(4,128)(2,1)S(1)}, u32[]{:S(2)}, u32[]{:S(2)}) async-start(bf16[32,4,5,128]{3,1,2,0:T(4,128)(2,1)} %copy.143), calls=%async_computation.1 | async-start | bytes 327680 | tf_op jit(solution)/shard_map/all_to_all | solution.py:193
  318.7 15.2 %all-to-all-done.1 = bf16[32,4,5,128]{3,1,2,0:T(4,128)(2,1)S(1)} async-done(((bf16[32,4,5,128]{3,1,2,0:T(4,128)(2,1)}), bf16[32,4,5,128]{3,1,2,0:T(4,128)(2,1)S(1)}, u32[]{:S(2)}, u32[]{:S(2)}) %all-to-all-start.1) | async-done | bytes 163872 | tf_op jit(solution)/shard_map/all_to_all | solution.py:193
  333.9 1.2 fusion.61
  335.0 1.2 fusion.62
  336.2 106.3 %all-reduce.3.cloned.1.call-done = (bf16[32,4,5,512]{3,0,2,1:T(8,128)(2,1)}, bf16[32,4,5,512]{3,0,2,1:T(8,128)(2,1)}, bf16[192,512]{1,0:T(8,128)(2,1)}, bf16[192,512]{1,0:T(8,128)(2,1)}) async-done(((bf16[32,4,5,512]{3,0,2,1:T(8,128)(2,1)}, bf16[32,4,5,512]{3,0,2,1:T(8,128)(2,1)}, bf16[192,512]{1,0:T(8,128)(2,1)}, bf16[192,512]{1,0:T(8,128)(2,1)}), (bf16[32,4,5,512]{3,0,2,1:T(8,128)(2,1)}, ...) | async-done | bytes 1703952 | tf_op jit(solution)/shard_map/psum | solution.py:197
  442.6 1.8 fusion.71
  445.2 14.6 %all-to-all-start.2 = ((bf16[32,4,5,128]{3,1,2,0:T(4,128)(2,1)}), bf16[32,4,5,128]{3,1,2,0:T(4,128)(2,1)S(1)}, u32[]{:S(2)}, u32[]{:S(2)}) async-start(bf16[32,4,5,128]{3,1,2,0:T(4,128)(2,1)} %copy.146), calls=%async_computation.2 | async-start | bytes 327680 | tf_op jit(solution)/shard_map/all_to_all | solution.py:200
  460.5 16.5 %all-to-all-done.2 = bf16[32,4,5,128]{3,1,2,0:T(4,128)(2,1)S(1)} async-done(((bf16[32,4,5,128]{3,1,2,0:T(4,128)(2,1)}), bf16[32,4,5,128]{3,1,2,0:T(4,128)(2,1)S(1)}, u32[]{:S(2)}, u32[]{:S(2)}) %all-to-all-start.2) | async-done | bytes 163872 | tf_op jit(solution)/shard_map/all_to_all | solution.py:200
  477.1 1.4 gather_fusion
  478.6 1.1 multiply_reduce_fusion
  (126 shorter events, 17.8 us)
Async XLA Ops:
  6.5 100.0 %copy-start = (bf16[128,2048]{1,0:T(8,128)(2,1)S(1)}, bf16[128,2048]{1,0:T(8,128)(2,1)}, u32[]{:S(2)}) copy-start(bf16[128,2048]{1,0:T(8,128)(2,1)} %param.33) | copy-start | bytes 1572868
  6.5 6.6 %copy-start.6 = (bf16[192,128]{1,0:T(8,128)(2,1)S(1)}, bf16[192,128]{1,0:T(8,128)(2,1)}, u32[]{:S(2)}) copy-start(bf16[192,128]{1,0:T(8,128)(2,1)} %param.30) | copy-start | bytes 147460
  6.5 84.8 %all-gather.2.cloned.1.call-start = ((), (), s32[]{:S(2)}) async-start(), calls=%async_computation.3 | async-start | bytes 6488064 | tf_op jit(solution)/shard_map/all_gather | solution.py:138
  8.2 5.5 %copy-start.10 = (f32[192,2]{0,1:T(2,128)S(1)}, f32[192,2]{0,1:T(2,128)}, u32[]{:S(2)}) copy-start(f32[192,2]{0,1:T(2,128)} %param.31) | copy-start | bytes 4612
  15.2 84.8 %copy-start.17 = (bf16[192,128]{1,0:T(8,128)(2,1)S(1)}, bf16[192,128]{1,0:T(8,128)(2,1)}, u32[]{:S(2)}) copy-start(bf16[192,128]{1,0:T(8,128)(2,1)} %param.28) | copy-start | bytes 147460
  15.3 84.8 %copy-start.18 = (f32[192,1]{0,1:T(1,128)S(1)}, f32[192,1]{0,1:T(1,128)}, u32[]{:S(2)}) copy-start(f32[192,1]{0,1:T(1,128)} %param.32) | copy-start | bytes 2308
  106.5 1.0 copy-start.1
  109.0 7.4 %copy-start.8 = (s32[192,2]{0,1:T(2,128)S(1)}, s32[192,2]{0,1:T(2,128)}, u32[]{:S(2)}) copy-start(s32[192,2]{0,1:T(2,128)} %param.38) | copy-start | bytes 4612
  109.0 17.3 %all-to-all-start = ((bf16[16,192,128]{2,1,0:T(8,128)(2,1)}), bf16[16,192,128]{2,1,0:T(8,128)(2,1)S(1)}, u32[]{:S(2)}, u32[]{:S(2)}) async-start(bf16[16,192,128]{2,1,0:T(8,128)(2,1)} %bitcast.107), calls=%async_computation | async-start | bytes 1572864 | tf_op jit(solution)/shard_map/all_to_all | solution.py:19
  115.7 24.2 %copy-start.7 = (bf16[192,128]{1,0:T(8,128)(2,1)S(1)}, bf16[192,128]{1,0:T(8,128)(2,1)}, u32[]{:S(2)}) copy-start(bf16[192,128]{1,0:T(8,128)(2,1)} %param.35) | copy-start | bytes 147460
  115.7 24.2 %copy-start.12 = (f32[128]{0:T(128)S(1)}, f32[128]{0:T(128)}, u32[]{:S(2)}) copy-start(f32[128]{0:T(128)} %param.36) | copy-start | bytes 1540
  115.7 38.0 %copy-start.9 = (f32[128]{0:T(128)S(1)}, f32[128]{0:T(128)}, u32[]{:S(2)}) copy-start(f32[128]{0:T(128)} %param.37) | copy-start | bytes 1540
  116.4 200.3 %copy-start.4 = (bf16[128,512]{1,0:T(8,128)(2,1)S(1)}, bf16[128,512]{1,0:T(8,128)(2,1)}, u32[]{:S(2)}) copy-start(bf16[128,512]{1,0:T(8,128)(2,1)} %param.43) | copy-start | bytes 393220
  116.6 201.1 %copy-start.5 = (bf16[128,512]{1,0:T(8,128)(2,1)S(1)}, bf16[128,512]{1,0:T(8,128)(2,1)}, u32[]{:S(2)}) copy-start(bf16[128,512]{1,0:T(8,128)(2,1)} %param.44) | copy-start | bytes 393220
  126.4 207.4 %copy-start.2 = (bf16[4,128,512]{2,1,0:T(8,128)(2,1)S(1)}, bf16[4,128,512]{2,1,0:T(8,128)(2,1)}, u32[]{:S(2)}) copy-start(bf16[4,128,512]{2,1,0:T(8,128)(2,1)} %param.40) | copy-start | bytes 1572868
  154.0 181.0 %copy-start.3 = (bf16[4,128,512]{2,1,0:T(8,128)(2,1)S(1)}, bf16[4,128,512]{2,1,0:T(8,128)(2,1)}, u32[]{:S(2)}) copy-start(bf16[4,128,512]{2,1,0:T(8,128)(2,1)} %param.41) | copy-start | bytes 1572868
  154.9 179.0 %all-to-all-start.1 = ((bf16[32,4,5,128]{3,1,2,0:T(4,128)(2,1)}), bf16[32,4,5,128]{3,1,2,0:T(4,128)(2,1)S(1)}, u32[]{:S(2)}, u32[]{:S(2)}) async-start(bf16[32,4,5,128]{3,1,2,0:T(4,128)(2,1)} %copy.143), calls=%async_computation.1 | async-start | bytes 327680 | tf_op jit(solution)/shard_map/all_to_all | solution.py:193
  316.7 125.9 %all-reduce.3.cloned.1.call-start = ((), (), s32[]{:S(2)}) async-start(), calls=%async_computation.4 | async-start | bytes 3407872 | tf_op jit(solution)/shard_map/psum | solution.py:197
  335.0 107.6 %copy-start.13 = (bf16[4,512,128]{2,1,0:T(8,128)(2,1)S(1)}, bf16[4,512,128]{2,1,0:T(8,128)(2,1)}, u32[]{:S(2)}) copy-start(bf16[4,512,128]{2,1,0:T(8,128)(2,1)} %param.42) | copy-start | bytes 1572868
  442.6 17.7 %copy-start.11 = (f32[192,2]{0,1:T(2,128)S(1)}, f32[192,2]{0,1:T(2,128)}, u32[]{:S(2)}) copy-start(f32[192,2]{0,1:T(2,128)} %param.39) | copy-start | bytes 4612
  444.4 35.2 %copy-start.14 = (bf16[192,512]{1,0:T(8,128)(2,1)S(1)}, bf16[192,512]{1,0:T(8,128)(2,1)}, u32[]{:S(2)}) copy-start(bf16[192,512]{1,0:T(8,128)(2,1)} %get-tuple-element.401) | copy-start | bytes 589828
  444.5 35.2 %copy-start.15 = (bf16[192,512]{1,0:T(8,128)(2,1)S(1)}, bf16[192,512]{1,0:T(8,128)(2,1)}, u32[]{:S(2)}) copy-start(bf16[192,512]{1,0:T(8,128)(2,1)} %get-tuple-element.402) | copy-start | bytes 589828
  444.5 35.2 %copy-start.16 = (bf16[512,128]{1,0:T(8,128)(2,1)S(1)}, bf16[512,128]{1,0:T(8,128)(2,1)}, u32[]{:S(2)}) copy-start(bf16[512,128]{1,0:T(8,128)(2,1)} %param.45) | copy-start | bytes 393220
  445.2 31.7 %all-to-all-start.2 = ((bf16[32,4,5,128]{3,1,2,0:T(4,128)(2,1)}), bf16[32,4,5,128]{3,1,2,0:T(4,128)(2,1)S(1)}, u32[]{:S(2)}, u32[]{:S(2)}) async-start(bf16[32,4,5,128]{3,1,2,0:T(4,128)(2,1)} %copy.146), calls=%async_computation.2 | async-start | bytes 327680 | tf_op jit(solution)/shard_map/all_to_all | solution.py:200
Sparse Core Ops, SparseCore 0:
  9.5 81.8 all-gather.1
  336.4 106.1 all-reduce.2
where the time goes:
time: 491 us; the launch traced here: 487 us
  waiting for transfers between devices  224 us (46%)
  starting transfers between devices  183 us (37%)
  blocking collectives  26.9 us (5%)
  local copies, waits for them, and re-layouts  19.3 us (4%)
  matrix products  14.7 us (3%)
  between operations  13.9 us (3%)
    all_to_all x1, starting transfers between devices, shards(): lax.all_to_all(outgoing, 'sp', split_axis=0, concat_axis=0, tiled=True)  162 us
    psum x1, waiting for transfers between devices, shards(): up_pre = lax.psum(up_part.astype(jnp.bfloat16), TP).astype(jnp.float32)  106 us
    all_gather x1, waiting for transfers between devices, shards(): gathered = lax.all_gather(joined_local, 'sp', axis=0, tiled=True)  76.1 us
    psum x4, blocking collectives, by_axis(): x = lax.psum(x, axis)  26.9 us
    all_to_all x1, waiting for transfers between devices, shards(): lax.all_to_all(produced.astype(jnp.bfloat16), 'sp', split_axis=0, concat_...  16.5 us
    all_to_all x1, waiting for transfers between devices, shards(): lax.all_to_all(outgoing, 'sp', split_axis=0, concat_axis=0, tiled=True)  15.2 us
    all_to_all x1, starting transfers between devices, shards(): lax.all_to_all(produced.astype(jnp.bfloat16), 'sp', split_axis=0, concat_...  14.6 us
  transfers between devices with their start and end apart: 5, of which 5 were waited for; matrix products, arithmetic and copies ran while one was open for 2% of the time, Pallas kernels for 0%

commit v1 on v0

--- a/solution.py
+++ b/solution.py
@@ -7,6 +7,13 @@
 D = 2048
 TP = ("tp_0", "tp_1")
 epsilon = 1e-06
+
+
+def swapped_in(x, axis, dim):
+    size = lax.axis_size(axis)
+    blocks = jnp.stack([x for _ in range(size)])
+    blocks = lax.all_to_all(blocks, axis, split_axis=0, concat_axis=0)
+    return jnp.concatenate(blocks, axis=dim)
 
 
 def cut_along(x, dim, size):
@@ -135,7 +142,7 @@
     state = stick_block(
         empty_state(rows, heads_a, size_a, heads_b, size_b), queries, unpack(joined_local), causal
     )
-    gathered = lax.all_gather(joined_local, "sp", axis=0, tiled=True)
+    gathered = swapped_in(joined_local, "sp", 0)
 
     def turn(step, inner_state):
         start = jnp.maximum(position - step, 0) * rows

time: 491 us -> 698 us (1.42)
  waiting for transfers between devices: 224 us -> 419 us
  starting transfers between devices: 183 us -> 196 us
    all_to_all x0 -> x1, waiting for transfers between devices: none -> 271 us  [swapped_in(): blocks = lax.all_to_all(blocks, axis, split_axis=0, concat_axis=0)]
    all_gather x1 -> x0, waiting for transfers between devices: 76.1 us -> none  [shards(): gathered = lax.all_gather(joined_local, 'sp', axis=0, tiled=True)]
    all_to_all x0 -> x1, starting transfers between devices: none -> 16.9 us  [swapped_in(): blocks = lax.all_to_all(blocks, axis, split_axis=0, concat_axis=0)]
  transfers between devices with their start and end apart: 5 -> 5, of which waited for: 5 -> 5; matrix products, arithmetic and copies ran while one was open for 2% -> 1% of each run, Pallas kernels for 0% -> 0%
where the time goes in v1:
time: 698 us; the launch traced here: 694 us
  waiting for transfers between devices  419 us (60%)
  starting transfers between devices  196 us (28%)
  blocking collectives  26.9 us (4%)
  local copies, waits for them, and re-layouts  19.6 us (3%)
  between operations  13.9 us (2%)
  matrix products  13.8 us (2%)
    all_to_all x1, waiting for transfers between devices, swapped_in(): blocks = lax.all_to_all(blocks, axis, split_axis=0, concat_axis=0)  271 us
    all_to_all x1, starting transfers between devices, shards(): lax.all_to_all(outgoing, 'sp', split_axis=0, concat_axis=0, tiled=True)  157 us
    psum x1, waiting for transfers between devices, shards(): up_pre = lax.psum(up_part.astype(jnp.bfloat16), TP).astype(jnp.float32)  106 us
    psum x4, blocking collectives, by_axis(): x = lax.psum(x, axis)  26.9 us
    all_to_all x1, starting transfers between devices, swapped_in(): blocks = lax.all_to_all(blocks, axis, split_axis=0, concat_axis=0)  16.9 us
    all_to_all x1, waiting for transfers between devices, shards(): lax.all_to_all(produced.astype(jnp.bfloat16), 'sp', split_axis=0, concat_...  16.5 us
    all_to_all x1, waiting for transfers between devices, shards(): lax.all_to_all(outgoing, 'sp', split_axis=0, concat_axis=0, tiled=True)  15.2 us
    all_to_all x1, starting transfers between devices, shards(): lax.all_to_all(produced.astype(jnp.bfloat16), 'sp', split_axis=0, concat_...  14.6 us
  transfers between devices with their start and end apart: 5, of which 5 were waited for; matrix products, arithmetic and copies ran while one was open for 1% of the time, Pallas kernels for 0%

profile of v1, /device:TPU:1, one launch (start us, length us, event | category | flops | bytes accessed | tf_op | source)
XLA Modules:
  0.0 694.3 jit_solution(3236648173123781317)
XLA Ops:
  7.5 3.4 stack.2
  10.9 16.9 %all-to-all-start = ((bf16[32,192,512]{2,1,0:T(8,128)(2,1)}), bf16[32,192,512]{2,1,0:T(8,128)(2,1)}, u32[]{:S(2)}, u32[]{:S(2)}) async-start(bf16[32,192,512]{2,1,0:T(8,128)(2,1)} %stack.2), calls=%async_computation | async-start | bytes 12582912 | tf_op jit(solution)/shard_map/all_to_all | solution.py:15
  31.1 271.5 %all-to-all-done = bf16[32,192,512]{2,1,0:T(8,128)(2,1)} async-done(((bf16[32,192,512]{2,1,0:T(8,128)(2,1)}), bf16[32,192,512]{2,1,0:T(8,128)(2,1)}, u32[]{:S(2)}, u32[]{:S(2)}) %all-to-all-start) | async-done | bytes 6291488 | tf_op jit(solution)/shard_map/all_to_all | solution.py:15
  302.6 8.7 %copy.128 = bf16[6144,512]{0,1:T(8,128)(2,1)} copy(bf16[6144,512]{1,0:T(8,128)(2,1)} %bitcast.24) | data formatting | bytes 12582912 | tf_op jit(solution)/shard_map/while | solution.py:157
  311.3 6.4 while.19
  311.3 5.1 conditional.2
  313.5 1.3 fusion.43
  314.8 1.5 fusion.13
  320.2 6.8 all-to-all-start.1
  327.9 9.7 %all-to-all-done.1 = bf16[16,192,128]{2,1,0:T(8,128)(2,1)S(1)} async-done(((bf16[16,192,128]{2,1,0:T(8,128)(2,1)}), bf16[16,192,128]{2,1,0:T(8,128)(2,1)S(1)}, u32[]{:S(2)}, u32[]{:S(2)}) %all-to-all-start.1) | async-done | bytes 786464 | tf_op jit(solution)/shard_map/all_to_all | solution.py:26
  337.8 6.5 psum.56
  344.3 6.8 psum.57
  351.3 6.5 psum.58
  357.9 7.1 %psum.59 = f32[192]{0:T(256)S(1)} all-reduce(f32[192]{0:T(256)S(1)} %psum.58), channel_id=1, replica_groups=mesh['sp'=32,'tp_0'=4,'tp_1'=4] {'tp_1'}, use_global_device_ids=true, to_apply=%region_18.19 | all-reduce | flops 192 | bytes 1536 | tf_op jit(solution)/shard_map/psum | solution.py:32
  366.1 157.5 %all-to-all-start.2 = ((bf16[32,4,5,128]{3,1,2,0:T(4,128)(2,1)}), bf16[32,4,5,128]{3,1,2,0:T(4,128)(2,1)S(1)}, u32[]{:S(2)}, u32[]{:S(2)}) async-start(bf16[32,4,5,128]{3,1,2,0:T(4,128)(2,1)} %copy.137), calls=%async_computation.2 | async-start | bytes 327680 | tf_op jit(solution)/shard_map/all_to_all | solution.py:200
  525.5 15.2 %all-to-all-done.2 = bf16[32,4,5,128]{3,1,2,0:T(4,128)(2,1)S(1)} async-done(((bf16[32,4,5,128]{3,1,2,0:T(4,128)(2,1)}), bf16[32,4,5,128]{3,1,2,0:T(4,128)(2,1)S(1)}, u32[]{:S(2)}, u32[]{:S(2)}) %all-to-all-start.2) | async-done | bytes 163872 | tf_op jit(solution)/shard_map/all_to_all | solution.py:200
  540.7 1.2 fusion.61
  541.9 1.2 fusion.62
  543.1 106.4 %all-reduce.3.cloned.1.call-done = (bf16[32,4,5,512]{3,0,2,1:T(8,128)(2,1)}, bf16[32,4,5,512]{3,0,2,1:T(8,128)(2,1)}, bf16[192,512]{1,0:T(8,128)(2,1)}, bf16[192,512]{1,0:T(8,128)(2,1)}) async-done(((bf16[32,4,5,512]{3,0,2,1:T(8,128)(2,1)}, bf16[32,4,5,512]{3,0,2,1:T(8,128)(2,1)}, bf16[192,512]{1,0:T(8,128)(2,1)}, bf16[192,512]{1,0:T(8,128)(2,1)}), (bf16[32,4,5,512]{3,0,2,1:T(8,128)(2,1)}, ...) | async-done | bytes 1703952 | tf_op jit(solution)/shard_map/psum | solution.py:204
  649.5 1.8 fusion.71
  652.1 14.6 %all-to-all-start.3 = ((bf16[32,4,5,128]{3,1,2,0:T(4,128)(2,1)}), bf16[32,4,5,128]{3,1,2,0:T(4,128)(2,1)S(1)}, u32[]{:S(2)}, u32[]{:S(2)}) async-start(bf16[32,4,5,128]{3,1,2,0:T(4,128)(2,1)} %copy.140), calls=%async_computation.3 | async-start | bytes 327680 | tf_op jit(solution)/shard_map/all_to_all | solution.py:207
  667.3 16.5 %all-to-all-done.3 = bf16[32,4,5,128]{3,1,2,0:T(4,128)(2,1)S(1)} async-done(((bf16[32,4,5,128]{3,1,2,0:T(4,128)(2,1)}), bf16[32,4,5,128]{3,1,2,0:T(4,128)(2,1)S(1)}, u32[]{:S(2)}, u32[]{:S(2)}) %all-to-all-start.3) | async-done | bytes 163872 | tf_op jit(solution)/shard_map/all_to_all | solution.py:207
  684.0 1.4 gather_fusion
  685.4 1.1 multiply_reduce_fusion
  (134 shorter events, 16.0 us)
Async XLA Ops:
  6.5 311.2 %copy-start = (bf16[128,2048]{1,0:T(8,128)(2,1)S(1)}, bf16[128,2048]{1,0:T(8,128)(2,1)}, u32[]{:S(2)}) copy-start(bf16[128,2048]{1,0:T(8,128)(2,1)} %param.33) | copy-start | bytes 1572868
  10.9 17.3 %copy-start.8 = (bf16[192,128]{1,0:T(8,128)(2,1)S(1)}, bf16[192,128]{1,0:T(8,128)(2,1)}, u32[]{:S(2)}) copy-start(bf16[192,128]{1,0:T(8,128)(2,1)} %param.25) | copy-start | bytes 147460
  10.9 17.4 %copy-start.12 = (s32[192,2]{0,1:T(2,128)S(1)}, s32[192,2]{0,1:T(2,128)}, u32[]{:S(2)}) copy-start(s32[192,2]{0,1:T(2,128)} %param.38) | copy-start | bytes 4612
  10.9 17.8 %copy-start.9 = (bf16[192,128]{1,0:T(8,128)(2,1)S(1)}, bf16[192,128]{1,0:T(8,128)(2,1)}, u32[]{:S(2)}) copy-start(bf16[192,128]{1,0:T(8,128)(2,1)} %param.29) | copy-start | bytes 147460
  10.9 17.8 %copy-start.21 = (bf16[192,128]{1,0:T(8,128)(2,1)S(1)}, bf16[192,128]{1,0:T(8,128)(2,1)}, u32[]{:S(2)}) copy-start(bf16[192,128]{1,0:T(8,128)(2,1)} %param.28) | copy-start | bytes 147460
  10.9 17.8 %copy-start.22 = (f32[192,1]{0,1:T(1,128)S(1)}, f32[192,1]{0,1:T(1,128)}, u32[]{:S(2)}) copy-start(f32[192,1]{0,1:T(1,128)} %param.32) | copy-start | bytes 2308
  10.9 18.1 %copy-start.10 = (bf16[192,128]{1,0:T(8,128)(2,1)S(1)}, bf16[192,128]{1,0:T(8,128)(2,1)}, u32[]{:S(2)}) copy-start(bf16[192,128]{1,0:T(8,128)(2,1)} %param.30) | copy-start | bytes 147460
  10.9 291.6 %all-to-all-start = ((bf16[32,192,512]{2,1,0:T(8,128)(2,1)}), bf16[32,192,512]{2,1,0:T(8,128)(2,1)}, u32[]{:S(2)}, u32[]{:S(2)}) async-start(bf16[32,192,512]{2,1,0:T(8,128)(2,1)} %stack.2), calls=%async_computation | async-start | bytes 12582912 | tf_op jit(solution)/shard_map/all_to_all | solution.py:15
  320.2 17.4 %all-to-all-start.1 = ((bf16[16,192,128]{2,1,0:T(8,128)(2,1)}), bf16[16,192,128]{2,1,0:T(8,128)(2,1)S(1)}, u32[]{:S(2)}, u32[]{:S(2)}) async-start(bf16[16,192,128]{2,1,0:T(8,128)(2,1)} %bitcast.108), calls=%async_computation.1 | async-start | bytes 1572864 | tf_op jit(solution)/shard_map/all_to_all | solution.py:26
  326.9 24.2 %copy-start.11 = (bf16[192,128]{1,0:T(8,128)(2,1)S(1)}, bf16[192,128]{1,0:T(8,128)(2,1)}, u32[]{:S(2)}) copy-start(bf16[192,128]{1,0:T(8,128)(2,1)} %param.35) | copy-start | bytes 147460
  326.9 24.2 %copy-start.16 = (f32[128]{0:T(128)S(1)}, f32[128]{0:T(128)}, u32[]{:S(2)}) copy-start(f32[128]{0:T(128)} %param.36) | copy-start | bytes 1540
  326.9 38.0 %copy-start.13 = (f32[128]{0:T(128)S(1)}, f32[128]{0:T(128)}, u32[]{:S(2)}) copy-start(f32[128]{0:T(128)} %param.37) | copy-start | bytes 1540
  327.7 196.0 %copy-start.6 = (bf16[128,512]{1,0:T(8,128)(2,1)S(1)}, bf16[128,512]{1,0:T(8,128)(2,1)}, u32[]{:S(2)}) copy-start(bf16[128,512]{1,0:T(8,128)(2,1)} %param.43) | copy-start | bytes 393220
  327.9 196.7 %copy-start.7 = (bf16[128,512]{1,0:T(8,128)(2,1)S(1)}, bf16[128,512]{1,0:T(8,128)(2,1)}, u32[]{:S(2)}) copy-start(bf16[128,512]{1,0:T(8,128)(2,1)} %param.44) | copy-start | bytes 393220
  337.7 203.0 %copy-start.2 = (bf16[4,128,512]{2,1,0:T(8,128)(2,1)S(1)}, bf16[4,128,512]{2,1,0:T(8,128)(2,1)}, u32[]{:S(2)}) copy-start(bf16[4,128,512]{2,1,0:T(8,128)(2,1)} %param.40) | copy-start | bytes 1572868
  365.3 176.6 %copy-start.3 = (bf16[4,128,512]{2,1,0:T(8,128)(2,1)S(1)}, bf16[4,128,512]{2,1,0:T(8,128)(2,1)}, u32[]{:S(2)}) copy-start(bf16[4,128,512]{2,1,0:T(8,128)(2,1)} %param.41) | copy-start | bytes 1572868
  366.1 174.6 %all-to-all-start.2 = ((bf16[32,4,5,128]{3,1,2,0:T(4,128)(2,1)}), bf16[32,4,5,128]{3,1,2,0:T(4,128)(2,1)S(1)}, u32[]{:S(2)}, u32[]{:S(2)}) async-start(bf16[32,4,5,128]{3,1,2,0:T(4,128)(2,1)} %copy.137), calls=%async_computation.2 | async-start | bytes 327680 | tf_op jit(solution)/shard_map/all_to_all | solution.py:200
  523.6 125.9 %all-reduce.3.cloned.1.call-start = ((), (), s32[]{:S(2)}) async-start(), calls=%async_computation.4 | async-start | bytes 3407872 | tf_op jit(solution)/shard_map/psum | solution.py:204
  541.9 107.6 %copy-start.17 = (bf16[4,512,128]{2,1,0:T(8,128)(2,1)S(1)}, bf16[4,512,128]{2,1,0:T(8,128)(2,1)}, u32[]{:S(2)}) copy-start(bf16[4,512,128]{2,1,0:T(8,128)(2,1)} %param.42) | copy-start | bytes 1572868
  649.5 17.7 %copy-start.15 = (f32[192,2]{0,1:T(2,128)S(1)}, f32[192,2]{0,1:T(2,128)}, u32[]{:S(2)}) copy-start(f32[192,2]{0,1:T(2,128)} %param.39) | copy-start | bytes 4612
  651.3 35.2 %copy-start.18 = (bf16[192,512]{1,0:T(8,128)(2,1)S(1)}, bf16[192,512]{1,0:T(8,128)(2,1)}, u32[]{:S(2)}) copy-start(bf16[192,512]{1,0:T(8,128)(2,1)} %get-tuple-element.412) | copy-start | bytes 589828
  651.3 35.2 %copy-start.19 = (bf16[192,512]{1,0:T(8,128)(2,1)S(1)}, bf16[192,512]{1,0:T(8,128)(2,1)}, u32[]{:S(2)}) copy-start(bf16[192,512]{1,0:T(8,128)(2,1)} %get-tuple-element.413) | copy-start | bytes 589828
  651.4 35.2 %copy-start.20 = (bf16[512,128]{1,0:T(8,128)(2,1)S(1)}, bf16[512,128]{1,0:T(8,128)(2,1)}, u32[]{:S(2)}) copy-start(bf16[512,128]{1,0:T(8,128)(2,1)} %param.45) | copy-start | bytes 393220
  652.1 31.7 %all-to-all-start.3 = ((bf16[32,4,5,128]{3,1,2,0:T(4,128)(2,1)}), bf16[32,4,5,128]{3,1,2,0:T(4,128)(2,1)S(1)}, u32[]{:S(2)}, u32[]{:S(2)}) async-start(bf16[32,4,5,128]{3,1,2,0:T(4,128)(2,1)} %copy.140), calls=%async_computation.3 | async-start | bytes 327680 | tf_op jit(solution)/shard_map/all_to_all | solution.py:207
  (4 other events, 36.8 us)
Sparse Core Ops, SparseCore 0:
  543.2 106.2 all-reduce.2
